TPU v7x, 32 devices: a whole 2x2x4 slice. The times are simulated.
32 devices in a mesh: ep: 8 (over z, y), tp: 4 (over x, core).
Axes of the slice: x: 2, y: 2, z: 4, core: 2. Of those that a mesh axis runs over, the one named last changes fastest.
Arguments:
- cell_query_rows: bfloat16 [2048, 2048], P('ep', 'tp'), may hold values from -6 to 6
- cell_key_rows: bfloat16 [2048, 2048], P('ep', 'tp'), may hold values from -6 to 6
- cell_value_rows: bfloat16 [2048, 2048], P('ep', 'tp'), may hold values from -6 to 6
- output_gate_logits: bfloat16 [2048, 2048], P('ep', 'tp'), may hold values from -8 to 8
- log_input_gate: float32 [8, 2048], P('tp', 'ep'), may hold values from -4 to 110
- forget_gate_logits: float32 [8, 2048], P('tp', 'ep'), may hold values from -1 to 25
- extra_log_forget: float32 [8, 2048], P('tp', 'ep'), may hold values from -0.7 to 0
- cell_output_scale: float32 [2048], P('tp'), may hold values from 0.1 to 1.9
- tokens_into_experts: bfloat16 [4096, 2048], P(('ep', 'tp')), may hold values from -6 to 6
- expert_norm_scale: float32 [2048], replicated, may hold values from 0.1 to 1.9
- token_expert_index: int32 [4096, 2], P(('ep', 'tp')), may hold values from 0 to 7, all different within a row; in each aligned block of 128 rows (0 to 127, 128 to 255, ...) at most 40 rows name the same one
- chosen_expert_weight: float32 [4096, 2], P(('ep', 'tp')), may hold values from 0.3 to 3
- expert_gate_weight: bfloat16 [8, 2048, 3584], P('ep', None, 'tp'), may hold values from -0.125 to 0.125
- expert_up_weight: bfloat16 [8, 2048, 3584], P('ep', None, 'tp'), may hold values from -0.125 to 0.125
- expert_down_weight: bfloat16 [8, 3584, 2048], P('ep', 'tp'), may hold values from -0.09375 to 0.09375
Outputs:
- gated_head_output: bfloat16 [2048, 2048], P('ep', 'tp')
- expert_output: bfloat16 [4096, 2048], P(('ep', 'tp'))
Inputs may be any that keep to these rules, and one draw needn't show every extreme that they name: `token_expert_index`: each row names 2 different experts. Among the rows of one device (aligned blocks of 128 rows) no expert is named by more than 40 rows, and in every draw some expert is named by exactly 40 rows of some device.
All inputs are finite; a program needn't handle non-finite values.
Results may differ from a plain program's by a relative error of at most 0.012.
Values may be sent and summed in bfloat16 or wider, within the bound.
A program may use at most 128 MiB of HBM per device.

v0:
```python
import jax
import jax.numpy as jnp
from jax import lax
from jax.sharding import PartitionSpec as P

HEAD_DIM = 256
BLOCK = 64
TOPK = 2
EPSILON = 1e-06
PRECISE = lax.Precision.HIGHEST


def carried_in(x, axis, combine, identity):
    size, here = (lax.axis_size(axis), lax.axis_index(axis))
    everything = jax.tree.map(lambda part: lax.all_gather(part, axis), x)
    start = jax.tree.map(
        lambda part, zero: jnp.broadcast_to(jnp.asarray(zero, part.dtype), part.shape), x, identity
    )

    def step(k, before):
        reached = k < here
        new = combine(before, jax.tree.map(lambda part: part[k], everything))
        return jax.tree.map(lambda a, b: jnp.where(reached, a, b), new, before)

    return lax.fori_loop(0, size, step, start)


def combine(earlier, later):
    cell_early, norm_early, stab_early, total_early = earlier
    cell_late, norm_late, stab_late, total_late = later
    stabilizer = jnp.maximum(total_late + stab_early, stab_late)
    keep_factor = jnp.exp(total_late + stab_early - stabilizer)
    take_factor = jnp.exp(stab_late - stabilizer)
    cell_state = (
        keep_factor[..., None, None] * cell_early + take_factor[..., None, None] * cell_late
    )
    norm_state = keep_factor[..., None] * norm_early + take_factor[..., None] * norm_late
    return (cell_state, norm_state, stabilizer, total_early + total_late)


def mix_heads(
    cell_query_rows,
    cell_key_rows,
    cell_value_rows,
    output_gate_logits,
    log_input_gate,
    forget_gate_logits,
    extra_log_forget,
    cell_output_scale,
):
    n_tok, row_width = cell_query_rows.shape
    head_count = row_width // HEAD_DIM
    block_count = n_tok // BLOCK
    key_scale = HEAD_DIM ** (-0.5)
    block_shape = (block_count, BLOCK, head_count, HEAD_DIM)
    query_blocks = cell_query_rows.reshape(block_shape)
    key_blocks = cell_key_rows.reshape(block_shape)
    value_blocks = cell_value_rows.reshape(block_shape)
    gate_input = log_input_gate.reshape(head_count, block_count, BLOCK)
    forget_gate_value = (jax.nn.log_sigmoid(forget_gate_logits) + extra_log_forget).reshape(
        head_count, block_count, BLOCK
    )
    cumulative = jnp.cumsum(forget_gate_value, axis=-1)
    block_last = cumulative[..., -1]
    growth = block_last[..., None] - cumulative + gate_input
    block_top = jnp.max(growth, axis=-1)
    shares = jnp.exp(growth - block_top[..., None])
    key_float = key_blocks.astype(jnp.float32) * key_scale
    value_weighted = value_blocks.astype(jnp.float32) * shares.transpose(1, 2, 0)[..., None]
    cell_terms = jnp.einsum("bshv,bshk->bhvk", value_weighted, key_float, precision=PRECISE)
    norm_terms = jnp.einsum("hbs,bshk->bhk", shares, key_float, precision=PRECISE)
    block_terms = (cell_terms, norm_terms, block_top.T, block_last.T)
    identity_state = (
        jnp.zeros((head_count, HEAD_DIM, HEAD_DIM), jnp.float32),
        jnp.zeros((head_count, HEAD_DIM), jnp.float32),
        jnp.full((head_count,), -1e30, jnp.float32),
        jnp.zeros((head_count,), jnp.float32),
    )

    def fold_step(running, block_term):
        return (combine(running, block_term), running)

    device_total, before = lax.scan(fold_step, identity_state, block_terms)
    prior_state = carried_in(device_total, "ep", combine, identity_state)
    zero_state = (
        jnp.zeros((head_count, HEAD_DIM, HEAD_DIM), jnp.float32),
        jnp.zeros((head_count, HEAD_DIM), jnp.float32),
        jnp.zeros((head_count,), jnp.float32),
        jnp.zeros((head_count,), jnp.float32),
    )
    start_state = combine(zero_state, prior_state)
    cell_state, norm_state, stabilizer, _ = combine(start_state, before)
    inter_log = cumulative + stabilizer.T[:, :, None]
    causal = jnp.tril(jnp.ones((BLOCK, BLOCK), dtype=bool))
    spread = jnp.where(
        causal,
        cumulative[..., :, None] - cumulative[..., None, :] + gate_input[..., None, :],
        -jnp.inf,
    )
    row_top = jnp.maximum(inter_log, jnp.max(spread, axis=-1))
    intra_weight = jnp.exp(spread - row_top[..., None])
    inter_weight = jnp.exp(inter_log - row_top)
    scores = (
        jnp.einsum("bthd,bshd->hbts", query_blocks, key_blocks, preferred_element_type=jnp.float32)
        * key_scale
        * intra_weight
    )
    weights = scores.astype(jnp.bfloat16)
    numerator = jnp.einsum(
        "hbts,bshd->hbtd", weights, value_blocks, preferred_element_type=jnp.float32
    )
    query_float = query_blocks.astype(jnp.float32)
    numerator = numerator + inter_weight[..., None] * jnp.einsum(
        "bhvk,bthk->hbtv", cell_state, query_float, precision=PRECISE
    )
    denominator = jnp.sum(scores, axis=-1) + inter_weight * jnp.einsum(
        "bhk,bthk->hbt", norm_state, query_float, precision=PRECISE
    )
    cell_out = numerator / jnp.maximum(jnp.abs(denominator), 1.0)[..., None]
    cell_out = cell_out.transpose(1, 2, 0, 3).reshape(n_tok, row_width)
    return (
        cell_out * cell_output_scale * jax.nn.sigmoid(output_gate_logits.astype(jnp.float32))
    ).astype(jnp.bfloat16)


def slot_tables(ids, experts, capacity):
    flat_ids = ids.reshape(-1)
    onehot = (flat_ids[:, None] == jnp.arange(experts, dtype=jnp.int32)[None, :]).astype(jnp.int32)
    earlier = jnp.cumsum(onehot, axis=0) - onehot
    rank_in = jnp.sum(earlier * onehot, axis=1)
    slot_index = flat_ids * capacity + rank_in
    token_of = jnp.arange(flat_ids.shape[0], dtype=jnp.int32) // ids.shape[1]
    slot_hit = slot_index[:, None] == jnp.arange(experts * capacity, dtype=jnp.int32)[None, :]
    slot_owner = jnp.sum(jnp.where(slot_hit, token_of[:, None] + 1, 0), axis=0)
    return (slot_owner, slot_index.reshape(ids.shape))


def local(
    cell_query_rows,
    cell_key_rows,
    cell_value_rows,
    output_gate_logits,
    log_input_gate,
    forget_gate_logits,
    extra_log_forget,
    cell_output_scale,
    tokens_into_experts,
    expert_norm_scale,
    token_expert_index,
    chosen_expert_weight,
    expert_gate_weight,
    expert_up_weight,
    expert_down_weight,
):
    gated_head_output = mix_heads(
        cell_query_rows,
        cell_key_rows,
        cell_value_rows,
        output_gate_logits,
        log_input_gate,
        forget_gate_logits,
        extra_log_forget,
        cell_output_scale,
    )
    ep_count = lax.axis_size("ep")
    n_tok = tokens_into_experts.shape[0]
    experts = ep_count * expert_gate_weight.shape[0]
    capacity = n_tok * TOPK * 5 // (4 * experts)
    input_float = tokens_into_experts.astype(jnp.float32)
    normed = (
        input_float
        * lax.rsqrt(jnp.mean(input_float * input_float, axis=-1, keepdims=True) + EPSILON)
        * expert_norm_scale
    ).astype(jnp.bfloat16)
    gate_matrix = expert_gate_weight[0]
    up_matrix = expert_up_weight[0]
    down_matrix = expert_down_weight[0]
    slot_owner, slot_index = slot_tables(token_expert_index, experts, capacity)
    sendbuf = jnp.where(
        (slot_owner > 0)[:, None],
        normed[jnp.maximum(slot_owner - 1, 0)],
        jnp.zeros((), jnp.bfloat16),
    )
    arrived = lax.all_to_all(sendbuf, "ep", split_axis=0, concat_axis=0, tiled=True)
    routed_rows = lax.all_gather(arrived, "tp", axis=0, tiled=True)
    gate_out = jnp.dot(routed_rows, gate_matrix, preferred_element_type=jnp.float32)
    up_out = jnp.dot(routed_rows, up_matrix, preferred_element_type=jnp.float32)
    hidden = (jax.nn.silu(gate_out) * up_out).astype(jnp.bfloat16)
    summed = lax.psum_scatter(
        jnp.dot(hidden, down_matrix, preferred_element_type=jnp.float32).astype(jnp.bfloat16),
        "tp",
        scatter_dimension=0,
        tiled=True,
    )
    returned = lax.all_to_all(summed, "ep", split_axis=0, concat_axis=0, tiled=True)
    picked = returned[slot_index]
    expert_output = jnp.sum(
        chosen_expert_weight[..., None] * picked.astype(jnp.float32), axis=1
    ).astype(jnp.bfloat16)
    return (gated_head_output, expert_output)


def solution(mesh):
    return jax.shard_map(
        local,
        mesh=mesh,
        in_specs=(
            P("ep", "tp"),
            P("ep", "tp"),
            P("ep", "tp"),
            P("ep", "tp"),
            P("tp", "ep"),
            P("tp", "ep"),
            P("tp", "ep"),
            P("tp"),
            P(("ep", "tp"), None),
            P(),
            P(("ep", "tp"), None),
            P(("ep", "tp"), None),
            P("ep", None, "tp"),
            P("ep", None, "tp"),
            P("ep", "tp", None),
        ),
        out_specs=(P("ep", "tp"), P(("ep", "tp"), None)),
        check_vma=False,
    )
```

profile of v0, /device:TPU:0, one launch (start us, length us, event | category | flops | bytes accessed | tf_op | source)
XLA Modules:
  0.0 271.6 jit_solution(12901544852267951957)
XLA Ops:
  9.4 1.2 fusion.31
  10.8 1.2 fusion.33
  12.0 2.4 gather_fusion
  14.7 38.7 %all_to_all.21 = bf16[8,40,2048]{2,1,0:T(8,128)(2,1)} all-to-all(bf16[8,40,2048]{2,1,0:T(8,128)(2,1)S(1)} %broadcast_select_fusion.7), channel_id=1, replica_groups=mesh['ep'=8,'tp'=4] {'ep'}, dimensions={0} | all-to-all | bytes 2621440 | tf_op jit(solution)/shard_map/all_to_all | solution.py:184
  55.4 2.0 fusion.35
  57.4 4.8 %while.45 = (s32[]{:T(128)}, f32[2,256,256]{2,1,0:T(8,128)S(1)}, f32[2,256]{1,0:T(2,128)S(1)}, f32[2]{0:T(128)S(1)}, f32[2]{0:T(128)S(1)}, /*index=5*/f32[4,2,25...) while((s32[]{:T(128)}, f32[2,256,256]{2,1,0:T(8,128)S(1)}, ...), condition=%wide.region_3.4_spmd.clone, body=%wide.region_2.3_spmd.clone.sunk | while | flops 657939 | bytes 2632544 | solution.py:83
  63.0 30.0 %all-gather.8.cloned.1.call-done = bf16[1280,2048]{1,0:T(8,128)(2,1)} async-done(((bf16[320,2048]{1,0:T(8,128)(2,1)}), bf16[1280,2048]{1,0:T(8,128)(2,1)}) %all-gather.8.cloned.1.call-update) | async-done | bytes 5242896 | tf_op jit(solution)/shard_map/all_gather | solution.py:185
  93.0 10.0 %fusion.18 = f32[1280,896]{1,0:T(8,128)} fusion(bf16[1280,2048]{1,0:T(8,128)(2,1)} %all-gather.8.cloned.1.call-done, bf16[1,2048,896]{2,1,0:T(8,128)(2,1)} %param.31), kind=kOutput, calls=%fused_computation.43 | convolution fusion | flops 4697620480 | bytes 13500416 | tf_op jit(solution)/shard_map/dot_general | solution.py:186
  103.0 17.9 %convolution_convert_fusion = bf16[1280,2048]{1,0:T(8,128)(2,1)} fusion(bf16[1,896,2048]{2,1,0:T(8,128)(2,1)} %param.33, f32[1280,896]{1,0:T(8,128)} %fusion.18, bf16[1280,2048]{1,0:T(8,128)(2,1)} %all-gather.8.cloned.1.call-done, bf16[1,2048,896]{2,1,0:T(8,128)(2,1)} %param.32), kind=kOutput, calls=%fused_computation.39 | convolution fusion | flops 9404743680 | bytes 22413312 | tf_op jit(solution)/shard_map/dot_general | solution.py:190
  123.2 22.6 %all-reduce.2 = (f32[16]{0:T(128)S(1)}, f32[16]{0:T(128)S(1)}) all-reduce(f32[16]{0:T(128)S(1)} %dynamic-update-slice, f32[16]{0:T(128)S(1)} %dynamic-update-slice.1), channel_id=2, replica_groups=mesh['ep'=8,'tp'=4] {'ep'}, use_global_device_ids=true, to_apply=%add | all-reduce | flops 32 | bytes 256
  146.6 26.9 %all-gather.4 = f32[8,2,256]{2,1,0:T(2,128)S(1)} all-gather(f32[1,2,256]{2,1,0:T(2,128)S(1)} %bitcast.169), channel_id=5, replica_groups=mesh['ep'=8,'tp'=4] {'ep'}, dimensions={0}, use_global_device_ids=true | all-gather | bytes 18432 | tf_op jit(solution)/shard_map/all_gather | solution.py:15
  173.8 11.0 %while.46 = (s32[]{:T(128)}, f32[2,256,256]{2,1,0:T(8,128)S(1)}, f32[2,256]{1,0:T(2,128)S(1)}, f32[2]{0:T(128)S(1)}, f32[2]{0:T(128)S(1)}, /*index=5*/s32[]{:T(1...) while((s32[]{:T(128)}, f32[2,256,256]{2,1,0:T(8,128)S(1)}, ...), condition=%wide.region_5.6_spmd.clone, body=%wide.region_4.5_spmd.clone.sunk | while | flops 657944 | bytes 1579285 | solution.py:25
  175.2 1.3 fusion.92
  178.0 1.3 fusion.92
  179.4 1.3 fusion.92
  180.9 1.2 fusion.92
  182.2 1.2 fusion.92
  184.9 36.8 %reduce-scatter.2.cloned.1.call-done = bf16[320,2048]{1,0:T(8,128)(2,1)} async-done(((bf16[1280,2048]{1,0:T(8,128)(2,1)}), bf16[320,2048]{1,0:T(8,128)(2,1)}) %reduce-scatter.2.cloned.1.call-update) | async-done | bytes 1310736 | tf_op jit(solution)/shard_map/reduce_scatter | solution.py:189
  221.7 5.5 %all-to-all-start.1 = ((bf16[8,40,2048]{2,1,0:T(8,128)(2,1)}), bf16[8,40,2048]{2,1,0:T(8,128)(2,1)S(1)}, u32[]{:S(2)}, u32[]{:S(2)}) async-start(bf16[8,40,2048]{2,1,0:T(8,128)(2,1)} %bitcast.168), calls=%async_computation.2 | async-start | bytes 2621440 | tf_op jit(solution)/shard_map/all_to_all | solution.py:195
  229.1 1.5 fusion.27
  232.4 26.1 %all-to-all-done.1 = bf16[8,40,2048]{2,1,0:T(8,128)(2,1)S(1)} async-done(((bf16[8,40,2048]{2,1,0:T(8,128)(2,1)}), bf16[8,40,2048]{2,1,0:T(8,128)(2,1)S(1)}, u32[]{:S(2)}, u32[]{:S(2)}) %all-to-all-start.1) | async-done | bytes 1310752 | tf_op jit(solution)/shard_map/all_to_all | solution.py:195
  258.5 1.4 gather_fusion.1
  259.8 1.3 reshape.175
  261.2 3.9 %multiply_reduce_fusion = bf16[128,2048]{1,0:T(8,128)(2,1)} fusion(f32[128,2,2048]{2,1,0:T(2,128)S(1)} %reshape.175, f32[128,2]{1,0:T(8,128)S(1)} %copy.102), kind=kLoop, calls=%fused_computation.47 | loop fusion | flops 786432 | bytes 2622464 | tf_op jit(solution)/shard_map/reduce_sum | solution.py:197
  (173 shorter events, 20.7 us)
Async XLA Ops:
  7.2 85.9 %all-gather.8.cloned.1.call-start = ((), (), s32[]{:S(2)}) async-start(), calls=%async_computation.3 | async-start | bytes 6553600 | tf_op jit(solution)/shard_map/all_gather | solution.py:185
  14.6 38.9 %copy-start.8 = (f32[2,256]{1,0:T(2,128)S(1)}, f32[2,256]{1,0:T(2,128)}, u32[]{:S(2)}) copy-start(f32[2,256]{1,0:T(2,128)} %param.25) | copy-start | bytes 6148
  14.6 38.9 %copy-start.9 = (f32[2,256]{1,0:T(2,128)S(1)}, f32[2,256]{1,0:T(2,128)}, u32[]{:S(2)}) copy-start(f32[2,256]{1,0:T(2,128)} %param.24) | copy-start | bytes 6148
  14.6 39.0 %copy-start.10 = (f32[2,256]{1,0:T(2,128)S(1)}, f32[2,256]{1,0:T(2,128)}, u32[]{:S(2)}) copy-start(f32[2,256]{1,0:T(2,128)} %param.23) | copy-start | bytes 6148
  14.6 40.0 %copy-start.2 = (bf16[256,512]{1,0:T(8,128)(2,1)S(1)}, bf16[256,512]{1,0:T(8,128)(2,1)}, u32[]{:S(2)}) copy-start(bf16[256,512]{1,0:T(8,128)(2,1)} %param.20) | copy-start | bytes 786436
  14.7 40.1 %copy-start.3 = (bf16[256,512]{1,0:T(8,128)(2,1)S(1)}, bf16[256,512]{1,0:T(8,128)(2,1)}, u32[]{:S(2)}) copy-start(bf16[256,512]{1,0:T(8,128)(2,1)} %param.21) | copy-start | bytes 786436
  53.4 120.4 %all-gather.10.cloned.1.call-start = ((), (), s32[]{:S(2)}) async-start(), calls=%async_computation.5 | async-start | bytes 4718592 | tf_op jit(solution)/shard_map/all_gather | solution.py:15
  62.1 0.8 copy-start
  63.0 158.7 %reduce-scatter.2.cloned.1.call-start = ((), (), s32[]{:S(2)}) async-start(), calls=%async_computation.4 | async-start | bytes 6553600 | tf_op jit(solution)/shard_map/reduce_scatter | solution.py:189
  120.9 0.7 copy-start.12
  120.9 25.2 %copy-start.4 = (bf16[256,512]{1,0:T(8,128)(2,1)S(1)}, bf16[256,512]{1,0:T(8,128)(2,1)}, u32[]{:S(2)}) copy-start(bf16[256,512]{1,0:T(8,128)(2,1)} %param.19) | copy-start | bytes 786436
  120.9 25.4 %copy-start.6 = (s32[128,2]{0,1:T(2,128)S(1)}, s32[128,2]{0,1:T(2,128)}, u32[]{:S(2)}) copy-start(s32[128,2]{0,1:T(2,128)} %param.29) | copy-start | bytes 3076
  120.9 25.6 %copy-start.11 = (f32[128,2]{0,1:T(2,128)S(1)}, f32[128,2]{0,1:T(2,128)}, u32[]{:S(2)}) copy-start(f32[128,2]{0,1:T(2,128)} %param.30) | copy-start | bytes 3076
  221.7 36.8 %all-to-all-start.1 = ((bf16[8,40,2048]{2,1,0:T(8,128)(2,1)}), bf16[8,40,2048]{2,1,0:T(8,128)(2,1)S(1)}, u32[]{:S(2)}, u32[]{:S(2)}) async-start(bf16[8,40,2048]{2,1,0:T(8,128)(2,1)} %bitcast.168), calls=%async_computation.2 | async-start | bytes 2621440 | tf_op jit(solution)/shard_map/all_to_all | solution.py:195
  227.5 1.6 copy-start.1
  230.5 1.0 copy-start.5
  230.6 0.9 copy-start.7
Sparse Core Ops, SparseCore 0:
  53.5 39.4 all-gather.7
  95.7 73.2 all-gather.9
  171.5 50.1 reduce-scatter.1
where the time goes:
time: 272 us
  waiting for transfers between devices  93 us (34%)
  blocking collectives  88.2 us (32%)
  matrix products  32.6 us (12%)
  other arithmetic  25 us (9%)
  between operations  14.8 us (5%)
  local copies, waits for them, and re-layouts  12.1 us (4%)
  starting transfers between devices  5.64 us (2%)
    all_to_all x1, blocking collectives, local(): lax.all_to_all(sendbuf, 'ep', split_axis=0, concat_axis=0, tiled=True)  38.7 us
    reduce_scatter x1, waiting for transfers between devices, local(): lax.psum_scatter(jnp.dot(hidden, down_matrix, preferred_element_type=jnp....  36.8 us
    all_gather x1, waiting for transfers between devices, local(): routed_rows = lax.all_gather(arrived, 'tp', axis=0, tiled=True)  30 us
    all_gather x1, blocking collectives, carried_in(): everything = jax.tree.map(lambda part: lax.all_gather(part, axis), x)  26.9 us
    all_to_all x1, waiting for transfers between devices, local(): lax.all_to_all(summed, 'ep', split_axis=0, concat_axis=0, tiled=True)  26.1 us
    unnamed x1, blocking collectives  22.6 us
    dot_general x1, matrix products, local(): jnp.dot(hidden, down_matrix, preferred_element_type=jnp.float32)  17.9 us
    select_n x24, other arithmetic, step(): return jax.tree.map(lambda a, b: jnp.where(reached, a, b), new, before)  10.8 us
  transfers between devices with their start and end apart: 4, of which 3 were waited for; matrix products, arithmetic and copies ran while one was open for 20% of the time, Pallas kernels for 0%

commit v1 on v0

--- a/solution.py
+++ b/solution.py
@@ -182,7 +182,9 @@
         jnp.zeros((), jnp.bfloat16),
     )
     arrived = lax.all_to_all(sendbuf, "ep", split_axis=0, concat_axis=0, tiled=True)
-    routed_rows = lax.all_gather(arrived, "tp", axis=0, tiled=True)
+    routed_rows = jnp.concatenate(
+        lax.all_to_all(jnp.stack([arrived] * lax.axis_size("tp")), "tp", 0, 0), axis=0
+    )
     gate_out = jnp.dot(routed_rows, gate_matrix, preferred_element_type=jnp.float32)
     up_out = jnp.dot(routed_rows, up_matrix, preferred_element_type=jnp.float32)
     hidden = (jax.nn.silu(gate_out) * up_out).astype(jnp.bfloat16)

time: 272 us -> 254 us (0.934)
  blocking collectives: 88.2 us -> 45.8 us
  starting transfers between devices: 5.64 us -> 16 us
  waiting for transfers between devices: 93 us -> 99.6 us
  local copies, waits for them, and re-layouts: 12.1 us -> 16.5 us
    all_to_all x0 -> x2, waiting for transfers between devices: none -> 81.3 us  [the longest x1 53.8 us: local(): lax.all_to_all(jnp.stack([arrived] * lax.axis_size('tp')), 'tp', 0, 0)]
    all_to_all x1 -> x0, blocking collectives: 38.7 us -> none  [local(): lax.all_to_all(sendbuf, 'ep', split_axis=0, concat_axis=0, tiled=True)]
    reduce_scatter x1, waiting for transfers between devices: 36.8 us -> 0.03 us  [local(): lax.psum_scatter(jnp.dot(hidden, down_matrix, preferred_element_type=jnp....]
    all_gather x1 -> x0, waiting for transfers between devices: 30 us -> none  [local(): routed_rows = lax.all_gather(arrived, 'tp', axis=0, tiled=True)]
    all_to_all x0 -> x2, starting transfers between devices: none -> 12.3 us  [the longest x1 7.31 us: local(): lax.all_to_all(sendbuf, 'ep', split_axis=0, concat_axis=0, tiled=True)]
    all_to_all x1, waiting for transfers between devices: 26.1 us -> 18.2 us  [local(): lax.all_to_all(summed, 'ep', split_axis=0, concat_axis=0, tiled=True)]
    another operation x1 -> x2, local copies, waits for them, and re-layouts: 0.01 us -> 4.34 us  [the longest x1 4.34 us: local(): jnp.stack([arrived] * lax.axis_size('tp'))]
    unnamed x1, blocking collectives: 22.6 us -> 19.7 us
  transfers between devices with their start and end apart: 4 -> 5, of which waited for: 3 -> 3; matrix products, arithmetic and copies ran while one was open for 20% -> 21% of each run, Pallas kernels for 0% -> 0%
where the time goes in v1:
time: 254 us; the launch traced here: 253 us
  waiting for transfers between devices  99.6 us (39%)
  blocking collectives  45.8 us (18%)
  matrix products  32.3 us (13%)
  other arithmetic  25.7 us (10%)
  between operations  16.6 us (7%)
  local copies, waits for them, and re-layouts  16.5 us (6%)
  starting transfers between devices  16 us (6%)
    all_to_all x1, waiting for transfers between devices, local(): lax.all_to_all(jnp.stack([arrived] * lax.axis_size('tp')), 'tp', 0, 0)  53.8 us
    all_to_all x1, waiting for transfers between devices, local(): lax.all_to_all(sendbuf, 'ep', split_axis=0, concat_axis=0, tiled=True)  27.6 us
    all_gather x1, blocking collectives, carried_in(): everything = jax.tree.map(lambda part: lax.all_gather(part, axis), x)  26.1 us
    unnamed x1, blocking collectives  19.7 us
    all_to_all x1, waiting for transfers between devices, local(): lax.all_to_all(summed, 'ep', split_axis=0, concat_axis=0, tiled=True)  18.2 us
    dot_general x1, matrix products, local(): jnp.dot(hidden, down_matrix, preferred_element_type=jnp.float32)  17.6 us
    select_n x24, other arithmetic, step(): return jax.tree.map(lambda a, b: jnp.where(reached, a, b), new, before)  10.3 us
    dot_general x1, matrix products, local(): jnp.dot(routed_rows, gate_matrix, preferred_element_type=jnp.float32)  9.98 us
  transfers between devices with their start and end apart: 5, of which 3 were waited for; matrix products, arithmetic and copies ran while one was open for 21% of the time, Pallas kernels for 0%

profile of v1, /device:TPU:0, one launch (start us, length us, event | category | flops | bytes accessed | tf_op | source)
XLA Modules:
  0.0 252.6 jit_solution(15672609541801638965)
XLA Ops:
  10.2 1.2 fusion.31
  11.5 1.2 fusion.33
  12.8 2.4 gather_fusion
  15.3 1.2 broadcast_select_fusion.7
  16.5 7.3 %all-to-all-start = ((bf16[8,40,2048]{2,1,0:T(8,128)(2,1)}), bf16[8,40,2048]{2,1,0:T(8,128)(2,1)}, u32[]{:S(2)}, u32[]{:S(2)}) async-start(bf16[8,40,2048]{2,1,0:T(8,128)(2,1)} %broadcast_select_fusion.7), calls=%async_computation | async-start | bytes 2621440 | tf_op jit(solution)/shard_map/all_to_all | solution.py:184
  25.7 2.0 fusion.35
  27.7 27.6 %all-to-all-done = bf16[8,40,2048]{2,1,0:T(8,128)(2,1)} async-done(((bf16[8,40,2048]{2,1,0:T(8,128)(2,1)}), bf16[8,40,2048]{2,1,0:T(8,128)(2,1)}, u32[]{:S(2)}, u32[]{:S(2)}) %all-to-all-start) | async-done | bytes 1310752 | tf_op jit(solution)/shard_map/all_to_all | solution.py:184
  55.3 4.3 %stack.10 = bf16[4,320,2048]{2,1,0:T(8,128)(2,1)} broadcast(bf16[320,2048]{1,0:T(8,128)(2,1)} %bitcast.21), dimensions={1,2} | broadcast | bytes 6553600 | tf_op jit(solution)/shard_map/stack | solution.py:186
  59.7 5.0 %all-to-all-start.1 = ((bf16[4,320,2048]{2,1,0:T(8,128)(2,1)}), bf16[4,320,2048]{2,1,0:T(8,128)(2,1)}, u32[]{:S(2)}, u32[]{:S(2)}) async-start(bf16[4,320,2048]{2,1,0:T(8,128)(2,1)} %stack.10), calls=%async_computation.1 | async-start | bytes 10485760 | tf_op jit(solution)/shard_map/all_to_all | solution.py:186
  64.8 4.8 %while.45 = (s32[]{:T(128)}, f32[2,256,256]{2,1,0:T(8,128)S(1)}, f32[2,256]{1,0:T(2,128)S(1)}, f32[2]{0:T(128)S(1)}, f32[2]{0:T(128)S(1)}, /*index=5*/f32[4,2,25...) while((s32[]{:T(128)}, f32[2,256,256]{2,1,0:T(8,128)S(1)}, ...), condition=%wide.region_3.4_spmd.clone, body=%wide.region_2.3_spmd.clone.sunk | while | flops 657939 | bytes 2632544 | solution.py:83
  70.4 53.8 %all-to-all-done.1 = bf16[4,320,2048]{2,1,0:T(8,128)(2,1)} async-done(((bf16[4,320,2048]{2,1,0:T(8,128)(2,1)}), bf16[4,320,2048]{2,1,0:T(8,128)(2,1)}, u32[]{:S(2)}, u32[]{:S(2)}) %all-to-all-start.1) | async-done | bytes 5242912 | tf_op jit(solution)/shard_map/all_to_all | solution.py:186
  124.1 10.0 %fusion.18 = f32[1280,896]{1,0:T(8,128)} fusion(bf16[1280,2048]{1,0:T(8,128)(2,1)} %bitcast.22, bf16[1,2048,896]{2,1,0:T(8,128)(2,1)} %param.31), kind=kOutput, calls=%fused_computation.43 | convolution fusion | flops 4697620480 | bytes 13500416 | tf_op jit(solution)/shard_map/dot_general | solution.py:188
  134.1 17.6 %convolution_convert_fusion = bf16[1280,2048]{1,0:T(8,128)(2,1)} fusion(bf16[1,896,2048]{2,1,0:T(8,128)(2,1)} %param.33, f32[1280,896]{1,0:T(8,128)} %fusion.18, bf16[1280,2048]{1,0:T(8,128)(2,1)} %bitcast.22, bf16[1,2048,896]{2,1,0:T(8,128)(2,1)} %param.32), kind=kOutput, calls=%fused_computation.39 | convolution fusion | flops 9404743680 | bytes 22413312 | tf_op jit(solution)/shard_map/dot_general | solution.py:192
  154.0 19.7 %all-reduce.2 = (f32[16]{0:T(128)S(1)}, f32[16]{0:T(128)S(1)}) all-reduce(f32[16]{0:T(128)S(1)} %dynamic-update-slice, f32[16]{0:T(128)S(1)} %dynamic-update-slice.1), channel_id=2, replica_groups=mesh['ep'=8,'tp'=4] {'ep'}, use_global_device_ids=true, to_apply=%add | all-reduce | flops 32 | bytes 256
  174.6 26.1 %all-gather.4 = f32[8,2,256]{2,1,0:T(2,128)S(1)} all-gather(f32[1,2,256]{2,1,0:T(2,128)S(1)} %bitcast.169), channel_id=5, replica_groups=mesh['ep'=8,'tp'=4] {'ep'}, dimensions={0}, use_global_device_ids=true | all-gather | bytes 18432 | tf_op jit(solution)/shard_map/all_gather | solution.py:15
  201.0 10.5 %while.46 = (s32[]{:T(128)}, f32[2,256,256]{2,1,0:T(8,128)S(1)}, f32[2,256]{1,0:T(2,128)S(1)}, f32[2]{0:T(128)S(1)}, f32[2]{0:T(128)S(1)}, /*index=5*/s32[]{:T(1...) while((s32[]{:T(128)}, f32[2,256,256]{2,1,0:T(8,128)S(1)}, ...), condition=%wide.region_5.6_spmd.clone, body=%wide.region_4.5_spmd.clone.sunk | while | flops 657944 | bytes 1579285 | solution.py:25
  201.0 1.2 fusion.92
  202.3 1.2 fusion.92
  211.6 3.6 %all-to-all-start.2 = ((bf16[8,40,2048]{2,1,0:T(8,128)(2,1)}), bf16[8,40,2048]{2,1,0:T(8,128)(2,1)S(1)}, u32[]{:S(2)}, u32[]{:S(2)}) async-start(bf16[8,40,2048]{2,1,0:T(8,128)(2,1)} %bitcast.168), calls=%async_computation.3 | async-start | bytes 2621440 | tf_op jit(solution)/shard_map/all_to_all | solution.py:197
  217.0 1.5 fusion.27
  220.3 18.2 %all-to-all-done.2 = bf16[8,40,2048]{2,1,0:T(8,128)(2,1)S(1)} async-done(((bf16[8,40,2048]{2,1,0:T(8,128)(2,1)}), bf16[8,40,2048]{2,1,0:T(8,128)(2,1)S(1)}, u32[]{:S(2)}, u32[]{:S(2)}) %all-to-all-start.2) | async-done | bytes 1310752 | tf_op jit(solution)/shard_map/all_to_all | solution.py:197
  238.5 1.4 gather_fusion.1
  239.9 1.3 reshape.182
  241.2 3.9 %multiply_reduce_fusion = bf16[128,2048]{1,0:T(8,128)(2,1)} fusion(f32[128,2,2048]{2,1,0:T(2,128)S(1)} %reshape.182, f32[128,2]{1,0:T(8,128)S(1)} %copy.102), kind=kLoop, calls=%fused_computation.47 | loop fusion | flops 786432 | bytes 2622464 | tf_op jit(solution)/shard_map/reduce_sum | solution.py:199
  (174 shorter events, 24.0 us)
Async XLA Ops:
  15.2 8.7 %copy-start.8 = (f32[2,256]{1,0:T(2,128)S(1)}, f32[2,256]{1,0:T(2,128)}, u32[]{:S(2)}) copy-start(f32[2,256]{1,0:T(2,128)} %param.25) | copy-start | bytes 6148
  15.2 8.7 %copy-start.9 = (f32[2,256]{1,0:T(2,128)S(1)}, f32[2,256]{1,0:T(2,128)}, u32[]{:S(2)}) copy-start(f32[2,256]{1,0:T(2,128)} %param.24) | copy-start | bytes 6148
  15.3 8.8 %copy-start.10 = (f32[2,256]{1,0:T(2,128)S(1)}, f32[2,256]{1,0:T(2,128)}, u32[]{:S(2)}) copy-start(f32[2,256]{1,0:T(2,128)} %param.23) | copy-start | bytes 6148
  15.3 9.7 %copy-start.2 = (bf16[256,512]{1,0:T(8,128)(2,1)S(1)}, bf16[256,512]{1,0:T(8,128)(2,1)}, u32[]{:S(2)}) copy-start(bf16[256,512]{1,0:T(8,128)(2,1)} %param.20) | copy-start | bytes 786436
  15.3 9.8 %copy-start.3 = (bf16[256,512]{1,0:T(8,128)(2,1)S(1)}, bf16[256,512]{1,0:T(8,128)(2,1)}, u32[]{:S(2)}) copy-start(bf16[256,512]{1,0:T(8,128)(2,1)} %param.21) | copy-start | bytes 786436
  16.5 38.8 %all-to-all-start = ((bf16[8,40,2048]{2,1,0:T(8,128)(2,1)}), bf16[8,40,2048]{2,1,0:T(8,128)(2,1)}, u32[]{:S(2)}, u32[]{:S(2)}) async-start(bf16[8,40,2048]{2,1,0:T(8,128)(2,1)} %broadcast_select_fusion.7), calls=%async_computation | async-start | bytes 2621440 | tf_op jit(solution)/shard_map/all_to_all | solution.py:184
  59.7 64.5 %all-to-all-start.1 = ((bf16[4,320,2048]{2,1,0:T(8,128)(2,1)}), bf16[4,320,2048]{2,1,0:T(8,128)(2,1)}, u32[]{:S(2)}, u32[]{:S(2)}) async-start(bf16[4,320,2048]{2,1,0:T(8,128)(2,1)} %stack.10), calls=%async_computation.1 | async-start | bytes 10485760 | tf_op jit(solution)/shard_map/all_to_all | solution.py:186
  64.7 136.2 %all-gather.7.cloned.1.call-start = ((), (), s32[]{:S(2)}) async-start(), calls=%async_computation.5 | async-start | bytes 4718592 | tf_op jit(solution)/shard_map/all_gather | solution.py:15
  69.5 0.8 copy-start
  70.3 141.2 %reduce-scatter.2.cloned.1.call-start = ((), (), s32[]{:S(2)}) async-start(), calls=%async_computation.4 | async-start | bytes 6553600 | tf_op jit(solution)/shard_map/reduce_scatter | solution.py:191
  151.7 0.7 copy-start.12
  151.7 22.3 %copy-start.4 = (bf16[256,512]{1,0:T(8,128)(2,1)S(1)}, bf16[256,512]{1,0:T(8,128)(2,1)}, u32[]{:S(2)}) copy-start(bf16[256,512]{1,0:T(8,128)(2,1)} %param.19) | copy-start | bytes 786436
  151.7 22.5 %copy-start.6 = (s32[128,2]{0,1:T(2,128)S(1)}, s32[128,2]{0,1:T(2,128)}, u32[]{:S(2)}) copy-start(s32[128,2]{0,1:T(2,128)} %param.29) | copy-start | bytes 3076
  151.7 22.8 %copy-start.11 = (f32[128,2]{0,1:T(2,128)S(1)}, f32[128,2]{0,1:T(2,128)}, u32[]{:S(2)}) copy-start(f32[128,2]{0,1:T(2,128)} %param.30) | copy-start | bytes 3076
  211.6 26.9 %all-to-all-start.2 = ((bf16[8,40,2048]{2,1,0:T(8,128)(2,1)}), bf16[8,40,2048]{2,1,0:T(8,128)(2,1)S(1)}, u32[]{:S(2)}, u32[]{:S(2)}) async-start(bf16[8,40,2048]{2,1,0:T(8,128)(2,1)} %bitcast.168), calls=%async_computation.3 | async-start | bytes 2621440 | tf_op jit(solution)/shard_map/all_to_all | solution.py:197
  215.4 1.6 copy-start.1
  218.5 1.0 copy-start.5
  218.5 0.9 copy-start.7
Sparse Core Ops, SparseCore 0:
  70.5 72.2 all-gather.6
Sparse Core Ops, SparseCore 1:
  151.8 49.3 reduce-scatter.1
